TPU v7x, 32 devices: a whole 2x2x4 slice. The times are simulated.
32 devices in a mesh: tp: 16 (over z, y, x), dp: 2 (over core).
Axes of the slice: x: 2, y: 2, z: 4, core: 2. Of those that a mesh axis runs over, the one named last changes fastest.
Arguments:
- residual_in: bfloat16 [24, 4096], P(None, ('dp', 'tp')), may hold values from -40 to 40
- norm_gain: float32 [2, 4096], P(None, 'dp'), may hold values from 0.1 to 1.9
- w_query: bfloat16 [2, 4096, 4096], P(None, 'tp', 'dp'), may hold values from -0.09375 to 0.09375
- w_key: bfloat16 [2, 4096, 4096], P(None, 'tp', 'dp'), may hold values from -0.09375 to 0.09375
- w_value: bfloat16 [2, 4096, 4096], P(None, 'tp', 'dp'), may hold values from -0.09375 to 0.09375
- w_outgate: bfloat16 [2, 4096, 4096], P(None, 'tp', 'dp'), may hold values from -0.09375 to 0.09375
- w_igate: bfloat16 [2, 4096, 16], replicated, may hold values from -0.09375 to 0.09375
- w_fgate: bfloat16 [2, 4096, 16], replicated, may hold values from -0.09375 to 0.09375
- forget_bias: float32 [2, 16], replicated, may hold values from -1 to 4
- head_gain: float32 [2, 4096], P(None, 'tp'), may hold values from 0.1 to 1.9
- w_proj: bfloat16 [2, 4096, 4096], P(None, 'tp', 'dp'), may hold values from -0.125 to 0.125
- mem_matrix: float32 [2, 24, 4096, 256], P(None, 'dp', 'tp'), may hold values from -0.6 to 0.6
- mem_stab: float32 [2, 24, 16], P(None, 'dp'), may hold values from -4 to 4
Outputs:
- residual_out: bfloat16 [24, 4096], P(None, ('dp', 'tp'))
- mem_matrix_new: float32 [2, 24, 4096, 256], P(None, 'dp', 'tp')
- mem_stab_new: float32 [2, 24, 16], P(None, 'dp')
All inputs are finite; a program needn't handle non-finite values.
Results may differ from a plain program's by a relative error of at most 0.009.
Values may be sent and summed in bfloat16 or wider, within the bound.
A program may use at most 64 MiB of HBM per device.

v0:
```python
import jax
import jax.numpy as jnp
from jax import lax
from jax.sharding import PartitionSpec as P

D = 4096
HEAD_DIM = 256
BLOCKS = 2


epsilon = 1e-06


def swapped(block, axis, apart):
    count = lax.axis_size(axis)
    route = []
    for low in range(count):
        high = low | 1 << apart
        if high != low and high < count:
            route += [(low, high), (high, low)]
    return lax.ppermute(block, axis, route)


def gather_rows(own_rows):
    return lax.all_gather(own_rows, "tp", axis=1, tiled=True)


def finish_block(own_rows, partial_value):
    summed = lax.psum_scatter(partial_value, "tp", scatter_dimension=1, tiled=True)
    return (own_rows.astype(jnp.float32) + summed).astype(jnp.bfloat16)


def project_rows(scaled, weight_cols):
    return lax.dot_general(
        scaled, weight_cols, (((1,), (1,)), ((), ())), preferred_element_type=jnp.float32
    )


def memory_cell(
    layer_index,
    full_rows,
    norm_gain,
    w_query,
    w_key,
    w_value,
    w_outgate,
    w_igate,
    w_fgate,
    forget_bias,
    head_gain,
    w_proj,
    mem_matrix,
    mem_stab,
):
    tp_place = lax.axis_index("tp")
    dp_place = lax.axis_index("dp")
    col_width = w_query.shape[1]
    row_span = w_query.shape[2]
    group_size = HEAD_DIM // col_width
    head_index = tp_place // group_size
    rows_f = full_rows.astype(jnp.float32)
    scaled = (rows_f * norm_gain[layer_index][None, :]).astype(jnp.bfloat16)
    query_part = project_rows(scaled, w_query[layer_index])
    key_part = project_rows(scaled, w_key[layer_index])
    value_part = project_rows(scaled, w_value[layer_index])
    outgate_part = project_rows(scaled, w_outgate[layer_index])
    igate_rows = lax.dynamic_slice_in_dim(w_igate[layer_index], dp_place * row_span, row_span, 0)
    fgate_rows = lax.dynamic_slice_in_dim(w_fgate[layer_index], dp_place * row_span, row_span, 0)
    in_part = jnp.dot(scaled, igate_rows, preferred_element_type=jnp.float32)
    forget_part = jnp.dot(scaled, fgate_rows, preferred_element_type=jnp.float32)
    squares = jnp.sum(rows_f * rows_f, axis=1)
    query_cols, key_cols, value_cols, outgate, in_pre, forget_pre, square_sum = (
        lax.psum_scatter(query_part, "dp", scatter_dimension=0, tiled=True),
        lax.psum_scatter(key_part, "dp", scatter_dimension=0, tiled=True),
        lax.psum_scatter(value_part, "dp", scatter_dimension=0, tiled=True),
        lax.psum_scatter(outgate_part, "dp", scatter_dimension=0, tiled=True),
        lax.psum_scatter(in_part, "dp", scatter_dimension=0, tiled=True),
        lax.psum_scatter(forget_part, "dp", scatter_dimension=0, tiled=True),
        lax.psum_scatter(squares, "dp", scatter_dimension=0, tiled=True),
    )
    inv_rms = lax.rsqrt(square_sum / D + epsilon)
    row_scale = inv_rms[:, None]
    query_cols = row_scale * query_cols
    key_cols = row_scale * key_cols * HEAD_DIM ** (-0.5)
    value_cols = row_scale * value_cols
    outgate = row_scale * outgate
    in_gate = row_scale * in_pre
    log_forget = jax.nn.log_sigmoid(row_scale * forget_pre + forget_bias[layer_index][None, :])
    previous = mem_stab[layer_index]
    stab_new = jnp.maximum(log_forget + previous, in_gate)
    keep_weight = jnp.exp(log_forget + previous - stab_new)
    admit_weight = jnp.exp(in_gate - stab_new)
    keep_head = lax.dynamic_slice_in_dim(keep_weight, head_index, 1, 1)
    admit_head = lax.dynamic_slice_in_dim(admit_weight, head_index, 1, 1)
    paired = jnp.stack([query_cols, key_cols])
    for bit_index in range(group_size.bit_length() - 1):
        partner = swapped(paired, "tp", bit_index)
        is_upper = tp_place // (1 << bit_index) % 2 == 1
        paired = jnp.concatenate(
            [jnp.where(is_upper, partner, paired), jnp.where(is_upper, paired, partner)], axis=2
        )
    matrix = (
        keep_head[:, :, None] * mem_matrix[layer_index]
        + admit_head[:, :, None] * value_cols[:, :, None] * paired[1][:, None, :]
    )
    readout = jnp.einsum("bk,bvk->bv", paired[0], matrix, precision=lax.Precision.HIGHEST)
    energy = jnp.sum(readout * readout, axis=1)
    for bit_index in range(group_size.bit_length() - 1):
        energy = energy + swapped(energy, "tp", bit_index)
    normed = (
        readout * lax.rsqrt(energy / HEAD_DIM + epsilon)[:, None] * head_gain[layer_index][None, :]
    )
    gated_out = (jax.nn.sigmoid(outgate) * normed).astype(jnp.bfloat16)
    proj_rows = w_proj[layer_index]
    partial_value = jnp.dot(
        lax.all_gather(gated_out, "dp", axis=0, tiled=True),
        proj_rows,
        preferred_element_type=jnp.float32,
    )
    return (partial_value, matrix, stab_new)


def per_device(
    residual_in,
    norm_gain,
    w_query,
    w_key,
    w_value,
    w_outgate,
    w_igate,
    w_fgate,
    forget_bias,
    head_gain,
    w_proj,
    mem_matrix,
    mem_stab,
):
    own_rows = residual_in
    full_rows = gather_rows(own_rows)
    matrices = []
    stabs = []
    for layer_index in range(BLOCKS):
        partial_value, matrix, stab_new = memory_cell(
            layer_index,
            full_rows,
            norm_gain,
            w_query,
            w_key,
            w_value,
            w_outgate,
            w_igate,
            w_fgate,
            forget_bias,
            head_gain,
            w_proj,
            mem_matrix,
            mem_stab,
        )
        matrices.append(matrix)
        stabs.append(stab_new)
        if layer_index + 1 == BLOCKS:
            own_rows = finish_block(own_rows, partial_value)
        else:
            own_rows = finish_block(own_rows, partial_value)
            full_rows = gather_rows(own_rows)
    return (own_rows, jnp.stack(matrices), jnp.stack(stabs))


def solution(mesh):
    in_specs = (
        P(None, ("dp", "tp")),
        P(None, "dp"),
        P(None, "tp", "dp"),
        P(None, "tp", "dp"),
        P(None, "tp", "dp"),
        P(None, "tp", "dp"),
        P(),
        P(),
        P(),
        P(None, "tp"),
        P(None, "tp", "dp"),
        P(None, "dp", "tp", None),
        P(None, "dp", None),
    )
    out_specs = (P(None, ("dp", "tp")), P(None, "dp", "tp", None), P(None, "dp", None))
    return jax.shard_map(
        per_device, mesh=mesh, in_specs=in_specs, out_specs=out_specs, check_vma=False
    )
```

profile of v0, /device:TPU:0, one launch (start us, length us, event | category | flops | bytes accessed | tf_op | source)
XLA Modules:
  0.0 306.8 jit_solution(5851925658672434457)
XLA Ops:
  7.2 0.9 fusion.158
  8.2 43.2 %all_gather.12 = bf16[24,2048]{1,0:T(8,128)(2,1)S(1)} all-gather(bf16[24,128]{1,0:T(8,128)(2,1)} %param.13), channel_id=1, replica_groups=mesh['tp'=16,'dp'=2] {'tp'}, dimensions={1}, use_global_device_ids=true | all-gather | bytes 104448 | tf_op jit(solution)/shard_map/all_gather | solution.py:25
  51.3 1.7 fusion.44
  53.0 1.6 fusion.42
  54.6 1.6 fusion.40
  56.3 0.4 fusion.46
  56.8 0.2 fusion.66
  56.9 0.2 fusion.68
  57.1 3.4 %fusion.149 = (f32[16,256]{1,0:T(8,128)S(1)}, f32[16,256]{1,0:T(8,128)S(1)}, f32[16,16]{1,0:T(8,128)S(1)}, f32[16,16]{1,0:T(8,128)S(1)}, f32[16,256]{1,0:T(8,128)S(1)}, /*index=5*/f32[16,256]{1,0:T(8,128)S(1)}) fusion(f32[24,256]{1,0:T(8,128)S(1)} %fusion.40, f32[24,256]{1,0:T(8,128)S(1)} %fusion.42, f32[24,16]{1,0:T(8,128)S(1)} %fusion.68, ...), kind=kCustom, calls=%all-reduce-scatter.13 | all-reduce-scatter fusion | flops 33793 | bytes 169472
  60.4 2.1 collective-permute-start.3
  62.5 1.3 collective-permute-start.2
  63.8 1.3 collective-permute-start
  65.2 1.3 collective-permute-start.1
  66.5 1.3 collective-permute-start.4
  67.8 0.1 fusion.58
  68.0 2.5 all-reduce
  70.5 0.6 fusion.161
  72.4 2.1 collective-permute-start.5
  74.5 0.1 concatenate.3
  74.7 0.1 concatenate.2
  74.9 0.2 fusion.137
  75.1 0.1 concatenate.1
  75.3 0.1 concatenate.4
  75.5 0.1 concatenate.5
  75.7 4.7 %fusion.16 = f32[12,1,256]{2,1,0:T(1,128)S(1)} fusion(f32[2,12,256,256]{3,2,1,0:T(8,128)} %param.24, f32[12,256]{1,0:T(8,128)S(1)} %get-tuple-element.64, f32[12,256]{1,0:T(8,128)S(1)} %get-tuple-element.65, f32[12]{0:T(128)S(1)} %get-tuple-element.14, f32[12,256,1]{1,0,2:T(8,128)S(1)} %get-tuple-element.63), kind=kOutput, calls=%fused_computation.6 | convolution fusion | flops 11796480 | bytes 3194928 | tf_op jit(solution)/shard_map/bk,bvk->bv/dot_general | solution.py:106
  80.4 0.1 fusion.112
  80.6 0.1 concatenate
  80.8 1.8 all-gather
  82.6 0.9 fusion.38
  83.6 73.1 %reduce-scatter.27.cloned.1.call-done = f32[24,128]{1,0:T(8,128)} async-done(((f32[24,2048]{1,0:T(8,128)}), f32[24,128]{1,0:T(8,128)}) %reduce-scatter.27.cloned.1.call-update) | async-done | bytes 12304 | tf_op jit(solution)/shard_map/reduce_scatter | solution.py:29
  156.8 0.9 add_convert_fusion.1
  157.7 36.4 %all_gather.14 = bf16[24,2048]{1,0:T(8,128)(2,1)S(1)} all-gather(bf16[24,128]{1,0:T(8,128)(2,1)S(1)} %add_convert_fusion.1), channel_id=1, replica_groups=mesh['tp'=16,'dp'=2] {'tp'}, dimensions={1}, use_global_device_ids=true | all-gather | bytes 104448 | tf_op jit(solution)/shard_map/all_gather | solution.py:25
  194.1 0.1 fusion.60
  194.2 1.6 fusion.34
  195.8 1.6 fusion.32
  197.5 1.6 fusion.30
  199.1 0.4 fusion.36
  199.5 0.2 fusion.64
  199.7 0.2 fusion.62
  199.8 2.5 all-reduce.7
  202.4 3.3 %fusion.148 = (f32[16,256]{1,0:T(8,128)S(1)}, f32[16,256]{1,0:T(8,128)S(1)}, f32[16,16]{1,0:T(8,128)S(1)}, f32[16,16]{1,0:T(8,128)S(1)}, f32[16,256]{1,0:T(8,128)S(1)}, /*index=5*/f32[16,256]{1,0:T(8,128)S(1)}) fusion(f32[24,256]{1,0:T(8,128)S(1)} %fusion.30, f32[24,256]{1,0:T(8,128)S(1)} %fusion.32, f32[24,16]{1,0:T(8,128)S(1)} %fusion.64, ...), kind=kCustom, calls=%all-reduce-scatter.12 | all-reduce-scatter fusion | flops 33793 | bytes 169472
  205.8 2.1 collective-permute-start.9
  207.9 1.3 collective-permute-start.8
  209.2 1.3 collective-permute-start.6
  210.5 1.3 collective-permute-start.7
  211.8 1.3 collective-permute-start.10
  213.1 1.3 collective-permute-start.11
  214.4 0.1 concatenate.9
  214.5 0.1 concatenate.8
  214.7 0.1 fusion.150
  214.8 0.6 copy.24
  215.4 0.2 fusion.133
  215.6 0.1 concatenate.7
  215.8 0.1 concatenate.10
  215.9 0.1 concatenate.11
  216.2 4.7 %fusion.13 = f32[12,1,256]{2,1,0:T(1,128)S(1)} fusion(f32[2,12,256,256]{3,2,1,0:T(8,128)} %param.24, f32[12,256]{1,0:T(8,128)S(1)} %get-tuple-element.61, f32[12,256]{1,0:T(8,128)S(1)} %get-tuple-element.62, f32[12]{0:T(128)S(1)} %get-tuple-element.12, f32[12,256,1]{1,0,2:T(8,128)S(1)} %get-tuple-element.60), kind=kOutput, calls=%fused_computation.3 | convolution fusion | flops 11796480 | bytes 3194928 | tf_op jit(solution)/shard_map/bk,bvk->bv/dot_general | solution.py:106
  220.9 0.1 fusion.110
  221.0 0.1 concatenate.6
  221.3 1.8 all-gather.1
  223.1 0.9 fusion.28
  224.0 3.4 %multiply_add_fusion.1 = (f32[1,12,256,256]{3,2,1,0:T(8,128)S(1)}, f32[1,12,256,256]{3,2,1,0:T(8,128)S(1)}) fusion(f32[2,12,256,256]{3,2,1,0:T(8,128)} %param.24, f32[12,256]{1,0:T(8,128)S(1)} %get-tuple-element.64, f32[12,256]{1,0:T(8,128)S(1)} %get-tuple-element.65, f32[12]{0:T(128)S(1)} %get-tuple-element.14, f32[12,256]{1,0:T(8,128)S(1)} %get-tuple-element.61, ...), kind=kLoop, calls=%fused_computation.8 | loop fusion | flops 4718592 | bytes 12632160 | tf_op jit(solution)/shard_map/add | solution.py:103
  227.5 3.4 %pad_maximum_fusion = f32[2,12,256,256]{3,2,1,0:T(8,128)} fusion(f32[1,12,256,256]{3,2,1,0:T(8,128)S(1)} %get-tuple-element.47, f32[1,12,256,256]{3,2,1,0:T(8,128)S(1)} %get-tuple-element.46), kind=kLoop, calls=%fused_computation | loop fusion | flops 1572864 | bytes 12582912 | tf_op jit(solution)/shard_map/stack | solution.py:166
  230.8 67.8 %reduce-scatter.29.cloned.1.call-done = f32[24,128]{1,0:T(8,128)} async-done(((f32[24,2048]{1,0:T(8,128)}), f32[24,128]{1,0:T(8,128)}) %reduce-scatter.29.cloned.1.call-update) | async-done | bytes 12304 | tf_op jit(solution)/shard_map/reduce_scatter | solution.py:29
  298.6 1.3 add_convert_fusion
  (65 shorter events, 1.0 us)
Async XLA Ops:
  7.2 49.5 %copy-start.1 = (bf16[2,4096,16]{1,2,0:T(8,128)(2,1)S(1)}, bf16[2,4096,16]{1,2,0:T(8,128)(2,1)}, u32[]{:S(2)}) copy-start(bf16[2,4096,16]{1,2,0:T(8,128)(2,1)} %param.19) | copy-start | bytes 786436
  7.2 49.5 %copy-start.2 = (bf16[2,4096,16]{1,2,0:T(8,128)(2,1)S(1)}, bf16[2,4096,16]{1,2,0:T(8,128)(2,1)}, u32[]{:S(2)}) copy-start(bf16[2,4096,16]{1,2,0:T(8,128)(2,1)} %param.20) | copy-start | bytes 786436
  7.2 149.6 %reduce-scatter.27.cloned.1.call-start = ((), (), s32[]{:S(2)}) async-start(), calls=%async_computation.2 | async-start | bytes 208896 | tf_op jit(solution)/shard_map/reduce_scatter | solution.py:29
  7.2 49.0 %copy-start.8 = (bf16[2,256,2048]{2,1,0:T(8,128)(2,1)S(1)}, bf16[2,256,2048]{2,1,0:T(8,128)(2,1)}, u32[]{:S(2)}) copy-start(bf16[2,256,2048]{2,1,0:T(8,128)(2,1)} %param.18) | copy-start | bytes 6291460
  51.3 16.6 %copy-start.7 = (f32[2,16]{1,0:T(2,128)S(1)}, f32[2,16]{1,0:T(2,128)}, u32[]{:S(2)}) copy-start(f32[2,16]{1,0:T(2,128)} %param.21) | copy-start | bytes 388
  51.3 16.6 %copy-start.5 = (f32[2,256]{1,0:T(2,128)S(1)}, f32[2,256]{1,0:T(2,128)}, u32[]{:S(2)}) copy-start(f32[2,256]{1,0:T(2,128)} %param.22) | copy-start | bytes 6148
  51.3 16.6 %copy-start.4 = (f32[2,12,16]{2,0,1:T(2,128)S(1)}, f32[2,12,16]{2,0,1:T(2,128)}, u32[]{:S(2)}) copy-start(f32[2,12,16]{2,0,1:T(2,128)} %param.25) | copy-start | bytes 4612
  51.3 19.1 %copy-start.6 = (u32[32]{0:T(128)S(1)}, u32[32]{0:T(128)}, u32[]{:S(2)}) copy-start(u32[32]{0:T(128)} %constant.55) | copy-start | bytes 388
  56.3 26.4 %copy-start = (bf16[2,256,2048]{2,1,0:T(8,128)(2,1)S(1)}, bf16[2,256,2048]{2,1,0:T(8,128)(2,1)}, u32[]{:S(2)}) copy-start(bf16[2,256,2048]{2,1,0:T(8,128)(2,1)} %param.23) | copy-start | bytes 6291460
  56.7 100.0 %copy-start.3 = (bf16[24,128]{1,0:T(8,128)(2,1)S(1)}, bf16[24,128]{1,0:T(8,128)(2,1)}, u32[]{:S(2)}) copy-start(bf16[24,128]{1,0:T(8,128)(2,1)} %param.13) | copy-start | bytes 18436
  60.4 12.0 %collective-permute-start.3 = (f32[4,16]{1,0:T(4,128)S(1)}, f32[4,16]{1,0:T(4,128)S(1)}, u32[]{:S(2)}, u32[]{:S(2)}) collective-permute-start(f32[4,16]{1,0:T(4,128)S(1)} %slice.99), channel_id=1, source_target_pairs={{0,1},{2,3},{4,5},{6,7},{8,9},{10,11},{12,13},{14,15},{16,17},{18,... | collective-permute-start | bytes 776
  62.5 12.1 %collective-permute-start.2 = (f32[4,16]{1,0:T(4,128)S(1)}, f32[4,16]{1,0:T(4,128)S(1)}, u32[]{:S(2)}, u32[]{:S(2)}) collective-permute-start(f32[4,16]{1,0:T(4,128)S(1)} %slice.98), channel_id=1, source_target_pairs={{0,1},{2,3},{4,5},{6,7},{8,9},{10,11},{12,13},{14,15},{16,17},{18,... | collective-permute-start | bytes 776
  63.8 16.7 %collective-permute-start = (f32[4,256]{1,0:T(4,128)S(1)}, f32[4,256]{1,0:T(4,128)S(1)}, u32[]{:S(2)}, u32[]{:S(2)}) collective-permute-start(f32[4,256]{1,0:T(4,128)S(1)} %slice.96), channel_id=1, source_target_pairs={{0,1},{2,3},{4,5},{6,7},{8,9},{10,11},{12,13},{14,15},{16,17},{18,... | collective-permute-start | bytes 12296
  65.2 10.0 %collective-permute-start.1 = (f32[4,256]{1,0:T(4,128)S(1)}, f32[4,256]{1,0:T(4,128)S(1)}, u32[]{:S(2)}, u32[]{:S(2)}) collective-permute-start(f32[4,256]{1,0:T(4,128)S(1)} %slice.97), channel_id=1, source_target_pairs={{0,1},{2,3},{4,5},{6,7},{8,9},{10,11},{12,13},{14,15},{16,17},{18,... | collective-permute-start | bytes 12296
  66.5 8.8 %collective-permute-start.4 = (f32[4,256]{1,0:T(4,128)S(1)}, f32[4,256]{1,0:T(4,128)S(1)}, u32[]{:S(2)}, u32[]{:S(2)}) collective-permute-start(f32[4,256]{1,0:T(4,128)S(1)} %slice.100), channel_id=1, source_target_pairs={{0,1},{2,3},{4,5},{6,7},{8,9},{10,11},{12,13},{14,15},{16,17},{18,... | collective-permute-start | bytes 12296
  72.4 3.0 collective-permute-start.5
  83.6 215.0 %reduce-scatter.29.cloned.1.call-start = ((), (), s32[]{:S(2)}) async-start(), calls=%async_computation.3 | async-start | bytes 208896 | tf_op jit(solution)/shard_map/reduce_scatter | solution.py:29
  156.8 42.3 %copy-start.9 = (bf16[2,256,2048]{2,1,0:T(8,128)(2,1)S(1)}, bf16[2,256,2048]{2,1,0:T(8,128)(2,1)}, u32[]{:S(2)}) copy-start(bf16[2,256,2048]{2,1,0:T(8,128)(2,1)} %param.18) | copy-start | bytes 6291460
  205.8 7.3 %collective-permute-start.9 = (f32[4,16]{1,0:T(4,128)S(1)}, f32[4,16]{1,0:T(4,128)S(1)}, u32[]{:S(2)}, u32[]{:S(2)}) collective-permute-start(f32[4,16]{1,0:T(4,128)S(1)} %slice.105), channel_id=1, source_target_pairs={{0,1},{2,3},{4,5},{6,7},{8,9},{10,11},{12,13},{14,15},{16,17},{18,... | collective-permute-start | bytes 776
  207.9 6.7 %collective-permute-start.8 = (f32[4,16]{1,0:T(4,128)S(1)}, f32[4,16]{1,0:T(4,128)S(1)}, u32[]{:S(2)}, u32[]{:S(2)}) collective-permute-start(f32[4,16]{1,0:T(4,128)S(1)} %slice.104), channel_id=1, source_target_pairs={{0,1},{2,3},{4,5},{6,7},{8,9},{10,11},{12,13},{14,15},{16,17},{18,... | collective-permute-start | bytes 776
  209.2 11.9 %collective-permute-start.6 = (f32[4,256]{1,0:T(4,128)S(1)}, f32[4,256]{1,0:T(4,128)S(1)}, u32[]{:S(2)}, u32[]{:S(2)}) collective-permute-start(f32[4,256]{1,0:T(4,128)S(1)} %slice.102), channel_id=1, source_target_pairs={{0,1},{2,3},{4,5},{6,7},{8,9},{10,11},{12,13},{14,15},{16,17},{18,... | collective-permute-start | bytes 12296
  210.5 5.1 %collective-permute-start.7 = (f32[4,256]{1,0:T(4,128)S(1)}, f32[4,256]{1,0:T(4,128)S(1)}, u32[]{:S(2)}, u32[]{:S(2)}) collective-permute-start(f32[4,256]{1,0:T(4,128)S(1)} %slice.103), channel_id=1, source_target_pairs={{0,1},{2,3},{4,5},{6,7},{8,9},{10,11},{12,13},{14,15},{16,17},{18,... | collective-permute-start | bytes 12296
  211.8 4.0 %collective-permute-start.10 = (f32[4,256]{1,0:T(4,128)S(1)}, f32[4,256]{1,0:T(4,128)S(1)}, u32[]{:S(2)}, u32[]{:S(2)}) collective-permute-start(f32[4,256]{1,0:T(4,128)S(1)} %slice.106), channel_id=1, source_target_pairs={{0,1},{2,3},{4,5},{6,7},{8,9},{10,11},{12,13},{14,15},{16,17},{18,... | collective-permute-start | bytes 12296
  213.1 2.8 collective-permute-start.11
Sparse Core Ops, SparseCore 0:
  83.7 73.0 reduce-scatter.26
  224.2 74.3 reduce-scatter.28
where the time goes:
time: 308 us; the launch traced here: 307 us
  waiting for transfers between devices  141 us (46%)
  blocking collectives  94.9 us (31%)
  matrix products  22.5 us (7%)
  starting transfers between devices  17.9 us (6%)
  between operations  15.9 us (5%)
  other arithmetic  10.5 us (3%)
  local copies, waits for them, and re-layouts  4 us (1%)
    reduce_scatter x2, waiting for transfers between devices, finish_block(): lax.psum_scatter(partial_value, 'tp', scatter_dimension=1, tiled=True)  141 us
    all_gather x2, blocking collectives, gather_rows(): return lax.all_gather(own_rows, 'tp', axis=1, tiled=True)  79.6 us
    unnamed x12, starting transfers between devices  17.8 us
    unnamed x4, blocking collectives  11.6 us
    dot_general x8, matrix products, project_rows(): lax.dot_general(scaled, weight_cols, (((1,), (1,)), ((), ())), preferred_...  10.5 us
    dot_general x2, matrix products, memory_cell(): jnp.einsum('bk,bvk->bv', paired[0], matrix, precision=lax.Precision.HIGHEST)  9.44 us
  transfers between devices with their start and end apart: 14, of which 2 were waited for; matrix products, arithmetic and copies ran while one was open for 7% of the time, Pallas kernels for 0%

commit v1 on v0

--- a/solution.py
+++ b/solution.py
@@ -1,6 +1,10 @@
+import functools
+
 import jax
 import jax.numpy as jnp
 from jax import lax
+from jax.experimental import pallas as pl
+from jax.experimental.pallas import tpu as pltpu
 from jax.sharding import PartitionSpec as P
 
 D = 4096
@@ -166,6 +170,342 @@
     return (own_rows, jnp.stack(matrices), jnp.stack(stabs))
 
 
+MESH = pl.DeviceIdType.MESH
+LANES = 128
+
+
+def flipped(place, count, step):
+    if count & (count - 1):
+        return lax.rem(place + step, count)
+    for bit in range(count.bit_length() - 1):
+        if step >> bit & 1:
+            place = place + (1 - 2 * (place // (1 << bit) % 2)) * (1 << bit)
+    return place
+
+
+def source_of(place, count, step):
+    if count & (count - 1):
+        return lax.rem(place + count - step, count)
+    return flipped(place, count, step)
+
+
+def fused_kernel(
+    n_tp,
+    n_dp,
+    seqs,
+    residual_ref,
+    gain_ref,
+    bias_ref,
+    head_gain_ref,
+    stab_ref,
+    wq_hbm,
+    wk_hbm,
+    wv_hbm,
+    wo_hbm,
+    wi_hbm,
+    wf_hbm,
+    wp_hbm,
+    mem_hbm,
+    out_ref,
+    stab_out_ref,
+    keep_out_ref,
+    value_out_ref,
+    key_out_ref,
+    w_in,
+    w_gate,
+    w_out,
+    mem,
+    mem_low,
+    rows,
+    scaled_buf,
+    partial_buf,
+    part_send,
+    part_recv,
+    gate_send,
+    gate_recv,
+    gated_all,
+    gated_rows,
+    sum_send,
+    sum_recv,
+    w_sem,
+    mem_sem,
+    rows_send_sem,
+    rows_recv_sem,
+    part_send_sem,
+    part_recv_sem,
+    gate_send_sem,
+    gate_recv_sem,
+    gated_send_sem,
+    gated_recv_sem,
+    sum_send_sem,
+    sum_recv_sem,
+):
+    me = lax.axis_index("tp")
+    core = lax.axis_index("dp")
+    width = residual_ref.shape[1]
+    share = seqs // n_dp
+    head_dim = mem.shape[-1]
+    span = n_tp * width
+    heads = bias_ref.shape[1]
+    pad = part_send.shape[2]
+
+    copies = {}
+
+    def fetch(name, src, dst, sem):
+        copies[name] = pltpu.make_async_copy(src, dst, sem)
+        copies[name].start()
+
+    def land(name):
+        copies.pop(name).wait()
+
+    row_start = pl.multiple_of(core * span, span)
+    for j in range(BLOCKS):
+        for i, w in enumerate((wq_hbm, wk_hbm, wv_hbm, wo_hbm)):
+            fetch(("in", j, i), w.at[j], w_in.at[j, i], w_sem.at[j, i])
+        for i, w in enumerate((wi_hbm, wf_hbm)):
+            fetch(
+                ("gate", j, i), w.at[j, pl.ds(row_start, span)], w_gate.at[j, i], w_sem.at[j, 4 + i]
+            )
+        fetch(("mem", j), mem_hbm.at[j], mem.at[j], mem_sem.at[j])
+        fetch(("out", j), wp_hbm.at[j], w_out.at[j], w_sem.at[j, 6])
+
+    barrier = pltpu.get_barrier_semaphore()
+    for step in range(n_tp - 1, 0, -1):
+        pl.semaphore_signal(
+            barrier, inc=1, device_id={"tp": flipped(me, n_tp, step)}, device_id_type=MESH
+        )
+    for step in range(1, n_dp):
+        pl.semaphore_signal(
+            barrier, inc=1, device_id={"dp": flipped(core, n_dp, step)}, device_id_type=MESH
+        )
+    rows[0, me] = residual_ref[...]
+    pl.semaphore_wait(barrier, n_tp - 1 + n_dp - 1)
+
+    own = residual_ref[...].astype(jnp.float32)
+    for j in range(BLOCKS):
+        sends = []
+        for step in range(n_tp - 1, 0, -1):
+            copy = pltpu.make_async_remote_copy(
+                src_ref=rows.at[j, me],
+                dst_ref=rows.at[j, me],
+                send_sem=rows_send_sem.at[j, step],
+                recv_sem=rows_recv_sem.at[j, step],
+                device_id={"tp": flipped(me, n_tp, step)},
+                device_id_type=MESH,
+            )
+            copy.start()
+            sends.append(copy)
+        land(("mem", j))
+        for b in range(share):
+            mem_low[j, b] = mem[j, b].astype(jnp.bfloat16)
+        for i in range(4):
+            land(("in", j, i))
+        for i in range(2):
+            land(("gate", j, i))
+        for copy in sends:
+            copy.wait()
+
+        squares = jnp.zeros((seqs, width), jnp.float32)
+        for t in range(n_tp):
+            chunk = rows[j, t].astype(jnp.float32)
+            squares = squares + chunk * chunk
+            cols = slice(t * width, (t + 1) * width)
+            scaled_buf[:, cols] = (chunk * gain_ref[j : j + 1, cols]).astype(jnp.bfloat16)
+        square_sum = jnp.sum(squares, axis=1, keepdims=True)
+        scaled = scaled_buf[...]
+        cols_in = 4 * head_dim
+        for i in range(2):
+            partial_buf[:, cols_in + i * LANES : cols_in + i * LANES + heads] = jnp.dot(
+                scaled, w_gate[j, i], preferred_element_type=jnp.float32
+            )
+        partial_buf[:, cols_in + 2 * LANES :] = jnp.broadcast_to(square_sum, (seqs, LANES))
+        for i in range(4):
+            partial_buf[:, i * head_dim : (i + 1) * head_dim] = lax.dot_general(
+                scaled, w_in[j, i], (((1,), (1,)), ((), ())), preferred_element_type=jnp.float32
+            )
+        for d in range(n_dp):
+            mine = partial_buf[d * share : (d + 1) * share, :]
+            gate_send[j, d, :share, :] = mine[:, cols_in:]
+            part_send[j, d, :share, :] = mine[:, :cols_in].astype(jnp.bfloat16)
+        sends = []
+        for step in range(1, n_dp):
+            target = flipped(core, n_dp, step)
+            for src, dst, send_sem, recv_sem in (
+                (part_send, part_recv, part_send_sem, part_recv_sem),
+                (gate_send, gate_recv, gate_send_sem, gate_recv_sem),
+            ):
+                copy = pltpu.make_async_remote_copy(
+                    src_ref=src.at[j, target],
+                    dst_ref=dst.at[j, step],
+                    send_sem=send_sem.at[j, step],
+                    recv_sem=recv_sem.at[j, step],
+                    device_id={"dp": target},
+                    device_id_type=MESH,
+                )
+                copy.start()
+                sends.append(copy)
+        sums = part_send[j, core, :share, :].astype(jnp.float32)
+        gates = gate_send[j, core, :share, :]
+        for copy in sends:
+            copy.wait()
+        for step in range(1, n_dp):
+            sums = sums + part_recv[j, step, :share, :].astype(jnp.float32)
+            gates = gates + gate_recv[j, step, :share, :]
+
+        inv_rms = lax.rsqrt(gates[:, 2 * LANES : 2 * LANES + 1] / D + epsilon)
+        query = inv_rms * sums[:, :head_dim]
+        key = inv_rms * sums[:, head_dim : 2 * head_dim] * HEAD_DIM ** (-0.5)
+        value = inv_rms * sums[:, 2 * head_dim : 3 * head_dim]
+        outgate = inv_rms * sums[:, 3 * head_dim : 4 * head_dim]
+        in_gate = inv_rms * gates[:, :heads]
+        forget_pre = inv_rms * gates[:, LANES : LANES + heads] + bias_ref[j : j + 1, :]
+        log_forget = jnp.minimum(forget_pre, 0.0) - jnp.log1p(jnp.exp(-jnp.abs(forget_pre)))
+        previous = stab_ref[j]
+        stab_new = jnp.maximum(log_forget + previous, in_gate)
+        stab_out_ref[j] = stab_new
+        keep_all = jnp.exp(log_forget + previous - stab_new)
+        admit_all = jnp.exp(in_gate - stab_new)
+        is_head = lax.broadcasted_iota(jnp.int32, (share, heads), 1) == me
+        keep = jnp.sum(jnp.where(is_head, keep_all, 0.0), axis=1, keepdims=True)
+        admit = jnp.sum(jnp.where(is_head, admit_all, 0.0), axis=1, keepdims=True)
+        admitted = admit * value
+        keep_out_ref[j] = jnp.broadcast_to(keep, (share, head_dim))
+        value_out_ref[j] = admitted
+        key_out_ref[j] = key
+        query_low = query.astype(jnp.bfloat16)
+        row_index = lax.broadcasted_iota(jnp.int32, (share, head_dim), 0)
+        recalled = jnp.zeros((share, head_dim), jnp.float32)
+        for b in range(share):
+            product = lax.dot_general(
+                query_low, mem_low[j, b], (((1,), (1,)), ((), ())), preferred_element_type=jnp.float32
+            )
+            recalled = jnp.where(row_index == b, product, recalled)
+        overlap = jnp.sum(query * key, axis=1, keepdims=True)
+        readout = keep * recalled + admitted * overlap
+        energy = jnp.sum(readout * readout, axis=1, keepdims=True)
+        normed = readout * lax.rsqrt(energy / HEAD_DIM + epsilon) * head_gain_ref[j : j + 1, :]
+        gated = normed / (1.0 + jnp.exp(-outgate))
+        gated_all[j, core, :share, :] = gated.astype(jnp.bfloat16)
+        sends = []
+        for step in range(1, n_dp):
+            copy = pltpu.make_async_remote_copy(
+                src_ref=gated_all.at[j, core],
+                dst_ref=gated_all.at[j, core],
+                send_sem=gated_send_sem.at[j, step],
+                recv_sem=gated_recv_sem.at[j, step],
+                device_id={"dp": flipped(core, n_dp, step)},
+                device_id_type=MESH,
+            )
+            copy.start()
+            sends.append(copy)
+        land(("out", j))
+        for copy in sends:
+            copy.wait()
+        for d in range(n_dp):
+            gated_rows[d * share : (d + 1) * share, :] = gated_all[j, d, :share, :].astype(jnp.float32)
+        gated_low = gated_rows[...].astype(jnp.bfloat16)
+        block_cols = 2 * width
+        for c in range(span // block_cols):
+            product = jnp.dot(
+                gated_low,
+                w_out[j, :, c * block_cols : (c + 1) * block_cols],
+                preferred_element_type=jnp.float32,
+            )
+            for part in range(2):
+                sum_send[j, 2 * c + part] = product[:, part * width : (part + 1) * width].astype(
+                    jnp.bfloat16
+                )
+        sends = []
+        for step in range(n_tp - 1, 0, -1):
+            target = flipped(me, n_tp, step)
+            copy = pltpu.make_async_remote_copy(
+                src_ref=sum_send.at[j, target],
+                dst_ref=sum_recv.at[j, step],
+                send_sem=sum_send_sem.at[j, step],
+                recv_sem=sum_recv_sem.at[j, step],
+                device_id={"tp": target},
+                device_id_type=MESH,
+            )
+            copy.start()
+            sends.append(copy)
+        total = sum_send[j, me].astype(jnp.float32)
+        for copy in sends:
+            copy.wait()
+        for step in range(1, n_tp):
+            total = total + sum_recv[j, step].astype(jnp.float32)
+        rounded = (own + total).astype(jnp.bfloat16)
+        if j + 1 < BLOCKS:
+            rows[j + 1, me] = rounded
+            own = rounded.astype(jnp.float32)
+        else:
+            out_ref[...] = rounded
+
+
+def fused_device(n_tp, n_dp, residual_in, norm_gain, w_query, w_key, w_value, w_outgate, w_igate,
+                 w_fgate, forget_bias, head_gain, w_proj, mem_matrix, mem_stab):
+    seqs, width = residual_in.shape
+    _, head_dim, span = w_query.shape
+    heads = w_igate.shape[2]
+    share = seqs // n_dp
+    pad = -(-share // 16) * 16
+    low, wide = jnp.bfloat16, jnp.float32
+    in_vmem = pl.BlockSpec(memory_space=pltpu.VMEM)
+    in_hbm = pl.BlockSpec(memory_space=pl.ANY)
+    per_block = lambda shape, dtype: pltpu.VMEM((BLOCKS,) + shape, dtype)
+    sems = lambda count: pltpu.SemaphoreType.DMA((BLOCKS, count))
+    out, stab_new, keep, value, key = pl.pallas_call(
+        functools.partial(fused_kernel, n_tp, n_dp, seqs),
+        out_shape=(
+            jax.ShapeDtypeStruct((seqs, width), low),
+            jax.ShapeDtypeStruct((BLOCKS, share, heads), wide),
+            jax.ShapeDtypeStruct((BLOCKS, share, head_dim), wide),
+            jax.ShapeDtypeStruct((BLOCKS, share, head_dim), wide),
+            jax.ShapeDtypeStruct((BLOCKS, share, head_dim), wide),
+        ),
+        in_specs=[in_vmem] * 5 + [in_hbm] * 8,
+        out_specs=[in_vmem] * 5,
+        scratch_shapes=[
+            per_block((4, head_dim, span), low),
+            per_block((2, span, heads), low),
+            per_block((head_dim, span), low),
+            per_block((share, head_dim, head_dim), wide),
+            per_block((share, head_dim, head_dim), low),
+            per_block((n_tp, seqs, width), low),
+            pltpu.VMEM((seqs, span), low),
+            pltpu.VMEM((seqs, 4 * head_dim + 3 * LANES), wide),
+            per_block((n_dp, pad, 4 * head_dim), low),
+            per_block((n_dp, pad, 4 * head_dim), low),
+            per_block((n_dp, pad, 3 * LANES), wide),
+            per_block((n_dp, pad, 3 * LANES), wide),
+            per_block((n_dp, pad, head_dim), low),
+            pltpu.VMEM((seqs, head_dim), wide),
+            per_block((n_tp, seqs, width), low),
+            per_block((n_tp, seqs, width), low),
+            sems(7),
+            pltpu.SemaphoreType.DMA((BLOCKS,)),
+            sems(n_tp),
+            sems(n_tp),
+            sems(n_dp),
+            sems(n_dp),
+            sems(n_dp),
+            sems(n_dp),
+            sems(n_dp),
+            sems(n_dp),
+            sems(n_tp),
+            sems(n_tp),
+        ],
+        compiler_params=pltpu.CompilerParams(collective_id=0, has_side_effects=True),
+        name="both_blocks",
+    )(
+        residual_in, norm_gain, forget_bias, head_gain, mem_stab,
+        w_query, w_key, w_value, w_outgate, w_igate, w_fgate, w_proj, mem_matrix,
+    )
+    matrix = (
+        keep[:, :, None, :] * mem_matrix + value[:, :, :, None] * key[:, :, None, :]
+    )
+    return out, matrix, stab_new
+
+
 def solution(mesh):
     in_specs = (
         P(None, ("dp", "tp")),
@@ -183,6 +523,25 @@
         P(None, "dp", None),
     )
     out_specs = (P(None, ("dp", "tp")), P(None, "dp", "tp", None), P(None, "dp", None))
-    return jax.shard_map(
-        per_device, mesh=mesh, in_specs=in_specs, out_specs=out_specs, check_vma=False
-    )
+    n_tp, n_dp = mesh.shape["tp"], mesh.shape["dp"]
+
+    def fits(residual_in, w_query):
+        width = residual_in.shape[1] // (n_tp * n_dp)
+        return (
+            w_query.shape[1] == n_tp * HEAD_DIM
+            and width % LANES == 0
+            and n_tp % 2 == 0
+            and residual_in.shape[0] % n_dp == 0
+        )
+
+    def run(residual_in, norm_gain, w_query, *others):
+        if fits(residual_in, w_query):
+            body = functools.partial(fused_device, n_tp, n_dp)
+        else:
+            body = per_device
+        step = jax.shard_map(
+            body, mesh=mesh, in_specs=in_specs, out_specs=out_specs, check_vma=False
+        )
+        return step(residual_in, norm_gain, w_query, *others)
+
+    return run

time: 308 us -> 51.8 us (0.17)
  waiting for transfers between devices: 141 us -> 0 us
  blocking collectives: 94.9 us -> 0 us
  Pallas kernels: 0 us -> 37.2 us
  matrix products: 22.5 us -> 0 us
  starting transfers between devices: 17.9 us -> 0 us
  between operations: 15.9 us -> 0.64 us
  other arithmetic: 10.5 us -> 5.11 us
  local copies, waits for them, and re-layouts: 4 us -> 8.43 us
    reduce_scatter x2 -> x0, waiting for transfers between devices: 141 us -> none  [finish_block(): lax.psum_scatter(partial_value, 'tp', scatter_dimension=1, tiled=True)]
    all_gather x4 -> x0, blocking collectives: 83.3 us -> none  [the longest x2 79.6 us: gather_rows(): return lax.all_gather(own_rows, 'tp', axis=1, tiled=True)]
    pallas_call x0 -> x1, Pallas kernels: none -> 37.2 us  [fused_device(): pl.pallas_call(functools.partial(fused_kernel, n_tp, n_dp, seqs), out_sha...]
    dot_general x16 -> x0, matrix products: 22.5 us -> none  [the longest x8 10.5 us: project_rows(): lax.dot_general(scaled, weight_cols, (((1,), (1,)), ((), ())), preferred_...]
    unnamed x12 -> x0, starting transfers between devices: 17.8 us -> none
    unnamed x4 -> x0, blocking collectives: 11.6 us -> none
    unnamed x48 -> x7, local copies, waits for them, and re-layouts: 3.04 us -> 8.43 us
    another operation x2 -> x0, other arithmetic: 3.36 us -> none  [per_device(): return (own_rows, jnp.stack(matrices), jnp.stack(stabs))]
  transfers between devices with their start and end apart: 14 -> 0, of which waited for: 2 -> 0; matrix products, arithmetic and copies ran while one was open for 7% -> 0% of each run, Pallas kernels for 0% -> 0%
where the time goes in v1:
time: 51.8 us; the launch traced here: 51.4 us
  Pallas kernels  37.2 us (72%)
  local copies, waits for them, and re-layouts  8.43 us (16%)
  other arithmetic  5.11 us (10%)
  between operations  0.64 us (1%)
    pallas_call x1, Pallas kernels, fused_device(): pl.pallas_call(functools.partial(fused_kernel, n_tp, n_dp, seqs), out_sha...  37.2 us
    unnamed x7, local copies, waits for them, and re-layouts  8.43 us
    add x1, other arithmetic, fused_device(): keep[:, :, None, :] * mem_matrix + value[:, :, :, None] * key[:, :, None, :]  5.11 us

profile of v1, /device:TPU:0, one launch (start us, length us, event | category | flops | bytes accessed | tf_op | source)
XLA Modules:
  0.0 51.4 jit_solution(14191640241089780415)
XLA Ops:
  0.6 1.3 %copy.16.stab_ref = f32[2,12,16]{2,1,0:T(8,128)} copy(f32[2,12,16]{2,0,1:T(2,128)} %param.25) | data formatting | bytes 3072 | tf_op args[12]
  1.9 2.6 %copy.17.wi_hbm = bf16[2,4096,16]{2,1,0:T(8,128)(2,1)} copy(bf16[2,4096,16]{1,2,0:T(8,128)(2,1)} %param.19) | data formatting | bytes 524288 | tf_op args[6]
  4.5 2.6 %copy.18.wf_hbm = bf16[2,4096,16]{2,1,0:T(8,128)(2,1)} copy(bf16[2,4096,16]{1,2,0:T(8,128)(2,1)} %param.20) | data formatting | bytes 524288 | tf_op args[7]
  7.1 37.2 %both_blocks.1 = (bf16[24,128]{1,0:T(8,128)(2,1)}, f32[2,12,16]{2,1,0:T(8,128)}, f32[2,12,256]{2,1,0:T(8,128)}, f32[2,12,256]{2,1,0:T(8,128)}, f32[2,12,256]{2,1,0:T(8,128)}) custom-call(bf16[24,128]{1,0:T(8,128)(2,1)} %residual_ref.1, f32[2,2048]{1,0:T(2,128)} %gain_ref.1, f32[2,16]{1,0:T(2,128)} %bias_ref.1, f32[2,256]{1,0:T(2,128)} %head_gain_ref.1, ...), custom_call_target="tpu_custom_call" | custom-call | tf_op jit(solution)/shard_map/both_blocks/pallas_call | solution.py:456
  44.3 1.3 %copy.19 = f32[2,12,16]{2,0,1:T(2,128)} copy(f32[2,12,16]{2,1,0:T(8,128)} %get-tuple-element.15) | data formatting | bytes 3072
  45.6 0.0 copy-start
  45.6 5.1 %multiply_add_fusion = f32[2,12,256,256]{3,2,1,0:T(8,128)} fusion(f32[2,12,256,256]{3,2,1,0:T(8,128)} %mem_hbm.1, f32[2,12,256]{2,1,0:T(8,128)} %get-tuple-element.11, f32[2,12,256]{2,1,0:T(8,128)} %get-tuple-element.10, f32[2,12,256]{2,1,0:T(8,128)} %get-tuple-element.9), kind=kLoop, calls=%fused_computation | loop fusion | flops 4718592 | bytes 12656640 | tf_op jit(solution)/shard_map/add | solution.py:504
  50.8 0.0 copy-done
  50.8 0.6 %copy.21 = bf16[24,128]{1,0:T(8,128)(2,1)} copy(bf16[24,128]{1,0:T(8,128)(2,1)S(1)} %copy-done) | data formatting | bytes 12288
Async XLA Ops:
  45.6 5.1 %copy-start = (bf16[24,128]{1,0:T(8,128)(2,1)S(1)}, bf16[24,128]{1,0:T(8,128)(2,1)}, u32[]{:S(2)}) copy-start(bf16[24,128]{1,0:T(8,128)(2,1)} %get-tuple-element.19) | copy-start | bytes 18436

commit v2 on v1

--- a/solution.py
+++ b/solution.py
@@ -183,12 +183,6 @@
     return place
 
 
-def source_of(place, count, step):
-    if count & (count - 1):
-        return lax.rem(place + count - step, count)
-    return flipped(place, count, step)
-
-
 def fused_kernel(
     n_tp,
     n_dp,
@@ -217,7 +211,6 @@
     mem,
     mem_low,
     rows,
-    scaled_buf,
     partial_buf,
     part_send,
     part_recv,
@@ -247,7 +240,6 @@
     head_dim = mem.shape[-1]
     span = n_tp * width
     heads = bias_ref.shape[1]
-    pad = part_send.shape[2]
 
     copies = {}
 
@@ -264,7 +256,10 @@
             fetch(("in", j, i), w.at[j], w_in.at[j, i], w_sem.at[j, i])
         for i, w in enumerate((wi_hbm, wf_hbm)):
             fetch(
-                ("gate", j, i), w.at[j, pl.ds(row_start, span)], w_gate.at[j, i], w_sem.at[j, 4 + i]
+                ("gate", j, i),
+                w.at[j, :, pl.ds(row_start, span)],
+                w_gate.at[j, pl.ds(i * heads, heads)],
+                w_sem.at[j, 4 + i],
             )
         fetch(("mem", j), mem_hbm.at[j], mem.at[j], mem_sem.at[j])
         fetch(("out", j), wp_hbm.at[j], w_out.at[j], w_sem.at[j, 6])
@@ -282,10 +277,11 @@
     pl.semaphore_wait(barrier, n_tp - 1 + n_dp - 1)
 
     own = residual_ref[...].astype(jnp.float32)
+    late_sends = []
     for j in range(BLOCKS):
-        sends = []
+        gather = {}
         for step in range(n_tp - 1, 0, -1):
-            copy = pltpu.make_async_remote_copy(
+            gather[step] = pltpu.make_async_remote_copy(
                 src_ref=rows.at[j, me],
                 dst_ref=rows.at[j, me],
                 send_sem=rows_send_sem.at[j, step],
@@ -293,8 +289,7 @@
                 device_id={"tp": flipped(me, n_tp, step)},
                 device_id_type=MESH,
             )
-            copy.start()
-            sends.append(copy)
+            gather[step].start()
         land(("mem", j))
         for b in range(share):
             mem_low[j, b] = mem[j, b].astype(jnp.bfloat16)
@@ -302,27 +297,28 @@
             land(("in", j, i))
         for i in range(2):
             land(("gate", j, i))
-        for copy in sends:
-            copy.wait()
-
-        squares = jnp.zeros((seqs, width), jnp.float32)
-        for t in range(n_tp):
-            chunk = rows[j, t].astype(jnp.float32)
+        squares = jnp.zeros((seqs, 2 * width), jnp.float32)
+        gate_sum = jnp.zeros((seqs, 2 * heads), jnp.float32)
+        in_sums = [jnp.zeros((seqs, head_dim), jnp.float32)] * 4
+        for step in range(n_tp // 2):
+            pair = flipped(me // 2, n_tp // 2, step)
+            for arrived in (2 * step, 2 * step + 1):
+                if arrived:
+                    gather[arrived].wait_recv()
+            chunk = jnp.concatenate([rows[j, 2 * pair], rows[j, 2 * pair + 1]], axis=1)
+            chunk = chunk.astype(jnp.float32)
             squares = squares + chunk * chunk
-            cols = slice(t * width, (t + 1) * width)
-            scaled_buf[:, cols] = (chunk * gain_ref[j : j + 1, cols]).astype(jnp.bfloat16)
+            cols = pl.ds(pl.multiple_of(pair * 2 * width, 2 * width), 2 * width)
+            scaled = (chunk * gain_ref[j : j + 1, cols]).astype(jnp.bfloat16)
+            gate_sum = gate_sum + project_rows(scaled, w_gate[j, :, cols])
+            for i in range(4):
+                in_sums[i] = in_sums[i] + project_rows(scaled, w_in[j, i, :, cols])
+        cols_in = 4 * head_dim
         square_sum = jnp.sum(squares, axis=1, keepdims=True)
-        scaled = scaled_buf[...]
-        cols_in = 4 * head_dim
-        for i in range(2):
-            partial_buf[:, cols_in + i * LANES : cols_in + i * LANES + heads] = jnp.dot(
-                scaled, w_gate[j, i], preferred_element_type=jnp.float32
-            )
-        partial_buf[:, cols_in + 2 * LANES :] = jnp.broadcast_to(square_sum, (seqs, LANES))
+        partial_buf[:, cols_in:] = jnp.broadcast_to(square_sum, (seqs, LANES))
+        partial_buf[:, cols_in : cols_in + 2 * heads] = gate_sum
         for i in range(4):
-            partial_buf[:, i * head_dim : (i + 1) * head_dim] = lax.dot_general(
-                scaled, w_in[j, i], (((1,), (1,)), ((), ())), preferred_element_type=jnp.float32
-            )
+            partial_buf[:, i * head_dim : (i + 1) * head_dim] = in_sums[i]
         for d in range(n_dp):
             mine = partial_buf[d * share : (d + 1) * share, :]
             gate_send[j, d, :share, :] = mine[:, cols_in:]
@@ -352,17 +348,17 @@
             sums = sums + part_recv[j, step, :share, :].astype(jnp.float32)
             gates = gates + gate_recv[j, step, :share, :]
 
-        inv_rms = lax.rsqrt(gates[:, 2 * LANES : 2 * LANES + 1] / D + epsilon)
+        inv_rms = lax.rsqrt(gates[:, 2 * heads : 2 * heads + 1] / D + epsilon)
         query = inv_rms * sums[:, :head_dim]
         key = inv_rms * sums[:, head_dim : 2 * head_dim] * HEAD_DIM ** (-0.5)
         value = inv_rms * sums[:, 2 * head_dim : 3 * head_dim]
         outgate = inv_rms * sums[:, 3 * head_dim : 4 * head_dim]
         in_gate = inv_rms * gates[:, :heads]
-        forget_pre = inv_rms * gates[:, LANES : LANES + heads] + bias_ref[j : j + 1, :]
+        forget_pre = inv_rms * gates[:, heads : 2 * heads] + bias_ref[j : j + 1, :]
         log_forget = jnp.minimum(forget_pre, 0.0) - jnp.log1p(jnp.exp(-jnp.abs(forget_pre)))
-        previous = stab_ref[j]
+        previous = stab_ref[:, j, :]
         stab_new = jnp.maximum(log_forget + previous, in_gate)
-        stab_out_ref[j] = stab_new
+        stab_out_ref[:, j, :] = stab_new
         keep_all = jnp.exp(log_forget + previous - stab_new)
         admit_all = jnp.exp(in_gate - stab_new)
         is_head = lax.broadcasted_iota(jnp.int32, (share, heads), 1) == me
@@ -404,41 +400,46 @@
         for d in range(n_dp):
             gated_rows[d * share : (d + 1) * share, :] = gated_all[j, d, :share, :].astype(jnp.float32)
         gated_low = gated_rows[...].astype(jnp.bfloat16)
-        block_cols = 2 * width
-        for c in range(span // block_cols):
-            product = jnp.dot(
-                gated_low,
-                w_out[j, :, c * block_cols : (c + 1) * block_cols],
-                preferred_element_type=jnp.float32,
-            )
+        scatter = {}
+
+        def send_pair(step):
+            for sent in (2 * step + 1, 2 * step):
+                if sent:
+                    target = flipped(me, n_tp, sent)
+                    scatter[sent] = pltpu.make_async_remote_copy(
+                        src_ref=sum_send.at[j, target],
+                        dst_ref=sum_recv.at[j, sent],
+                        send_sem=sum_send_sem.at[j, sent],
+                        recv_sem=sum_recv_sem.at[j, sent],
+                        device_id={"tp": target},
+                        device_id_type=MESH,
+                    )
+                    scatter[sent].start()
+
+        for step in range(n_tp // 2 - 1, -1, -1):
+            pair = flipped(me // 2, n_tp // 2, step)
+            cols = pl.ds(pl.multiple_of(pair * 2 * width, 2 * width), 2 * width)
+            product = jnp.dot(gated_low, w_out[j, :, cols], preferred_element_type=jnp.float32)
             for part in range(2):
-                sum_send[j, 2 * c + part] = product[:, part * width : (part + 1) * width].astype(
+                sum_send[j, 2 * pair + part] = product[:, part * width : (part + 1) * width].astype(
                     jnp.bfloat16
                 )
-        sends = []
-        for step in range(n_tp - 1, 0, -1):
-            target = flipped(me, n_tp, step)
-            copy = pltpu.make_async_remote_copy(
-                src_ref=sum_send.at[j, target],
-                dst_ref=sum_recv.at[j, step],
-                send_sem=sum_send_sem.at[j, step],
-                recv_sem=sum_recv_sem.at[j, step],
-                device_id={"tp": target},
-                device_id_type=MESH,
-            )
-            copy.start()
-            sends.append(copy)
-        total = sum_send[j, me].astype(jnp.float32)
-        for copy in sends:
-            copy.wait()
+            if step + 1 < n_tp // 2:
+                send_pair(step + 1)
+        send_pair(0)
+        total = own + sum_send[j, me].astype(jnp.float32)
         for step in range(1, n_tp):
+            scatter[step].wait_recv()
             total = total + sum_recv[j, step].astype(jnp.float32)
-        rounded = (own + total).astype(jnp.bfloat16)
+        late_sends += [*gather.values(), *scatter.values()]
+        rounded = total.astype(jnp.bfloat16)
         if j + 1 < BLOCKS:
             rows[j + 1, me] = rounded
             own = rounded.astype(jnp.float32)
         else:
             out_ref[...] = rounded
+    for copy in late_sends:
+        copy.wait_send()
 
 
 def fused_device(n_tp, n_dp, residual_in, norm_gain, w_query, w_key, w_value, w_outgate, w_igate,
@@ -457,7 +458,7 @@
         functools.partial(fused_kernel, n_tp, n_dp, seqs),
         out_shape=(
             jax.ShapeDtypeStruct((seqs, width), low),
-            jax.ShapeDtypeStruct((BLOCKS, share, heads), wide),
+            jax.ShapeDtypeStruct((share, BLOCKS, heads), wide),
             jax.ShapeDtypeStruct((BLOCKS, share, head_dim), wide),
             jax.ShapeDtypeStruct((BLOCKS, share, head_dim), wide),
             jax.ShapeDtypeStruct((BLOCKS, share, head_dim), wide),
@@ -466,17 +467,16 @@
         out_specs=[in_vmem] * 5,
         scratch_shapes=[
             per_block((4, head_dim, span), low),
-            per_block((2, span, heads), low),
+            per_block((2 * heads, span), low),
             per_block((head_dim, span), low),
             per_block((share, head_dim, head_dim), wide),
             per_block((share, head_dim, head_dim), low),
             per_block((n_tp, seqs, width), low),
-            pltpu.VMEM((seqs, span), low),
-            pltpu.VMEM((seqs, 4 * head_dim + 3 * LANES), wide),
+            pltpu.VMEM((seqs, 4 * head_dim + LANES), wide),
             per_block((n_dp, pad, 4 * head_dim), low),
             per_block((n_dp, pad, 4 * head_dim), low),
-            per_block((n_dp, pad, 3 * LANES), wide),
-            per_block((n_dp, pad, 3 * LANES), wide),
+            per_block((n_dp, pad, LANES), wide),
+            per_block((n_dp, pad, LANES), wide),
             per_block((n_dp, pad, head_dim), low),
             pltpu.VMEM((seqs, head_dim), wide),
             per_block((n_tp, seqs, width), low),
@@ -494,16 +494,24 @@
             sems(n_tp),
             sems(n_tp),
         ],
-        compiler_params=pltpu.CompilerParams(collective_id=0, has_side_effects=True),
+        compiler_params=pltpu.CompilerParams(
+            collective_id=0, has_side_effects=True
+        ),
+        cost_estimate=pl.CostEstimate(
+            flops=10 * BLOCKS * seqs * head_dim * span,
+            bytes_accessed=40 * BLOCKS * head_dim * span,
+            transcendentals=0,
+        ),
         name="both_blocks",
     )(
-        residual_in, norm_gain, forget_bias, head_gain, mem_stab,
-        w_query, w_key, w_value, w_outgate, w_igate, w_fgate, w_proj, mem_matrix,
+        residual_in, norm_gain, forget_bias, head_gain, mem_stab.transpose(1, 0, 2),
+        w_query, w_key, w_value, w_outgate, w_igate.swapaxes(1, 2), w_fgate.swapaxes(1, 2),
+        w_proj, mem_matrix,
     )
     matrix = (
         keep[:, :, None, :] * mem_matrix + value[:, :, :, None] * key[:, :, None, :]
     )
-    return out, matrix, stab_new
+    return out, matrix, stab_new.transpose(1, 0, 2)
 
 
 def solution(mesh):
@@ -525,17 +533,19 @@
     out_specs = (P(None, ("dp", "tp")), P(None, "dp", "tp", None), P(None, "dp", None))
     n_tp, n_dp = mesh.shape["tp"], mesh.shape["dp"]
 
-    def fits(residual_in, w_query):
+    def fits(residual_in, w_query, w_igate):
         width = residual_in.shape[1] // (n_tp * n_dp)
         return (
             w_query.shape[1] == n_tp * HEAD_DIM
             and width % LANES == 0
-            and n_tp % 2 == 0
+            and n_tp > 1
+            and n_tp & (n_tp - 1) == 0
+            and w_igate.shape[2] % 16 == 0
             and residual_in.shape[0] % n_dp == 0
         )
 
     def run(residual_in, norm_gain, w_query, *others):
-        if fits(residual_in, w_query):
+        if fits(residual_in, w_query, others[3]):
             body = functools.partial(fused_device, n_tp, n_dp)
         else:
             body = per_device

time: 51.8 us -> 43.1 us (0.83)
  local copies, waits for them, and re-layouts: 8.43 us -> 1.2 us
  Pallas kernels: 37.2 us -> 35.9 us
    unnamed x7 -> x6, local copies, waits for them, and re-layouts: 8.43 us -> 1.2 us
    pallas_call x1, Pallas kernels: 37.2 us -> 35.9 us  [fused_device(): pl.pallas_call(functools.partial(fused_kernel, n_tp, n_dp, seqs), out_sha...]
where the time goes in v2:
time: 43.1 us; the launch traced here: 42.9 us
  Pallas kernels  35.9 us (83%)
  other arithmetic  5.11 us (12%)
  local copies, waits for them, and re-layouts  1.2 us (3%)
  between operations  0.66 us (2%)
    pallas_call x1, Pallas kernels, fused_device(): pl.pallas_call(functools.partial(fused_kernel, n_tp, n_dp, seqs), out_sha...  35.9 us
    add x1, other arithmetic, fused_device(): keep[:, :, None, :] * mem_matrix + value[:, :, :, None] * key[:, :, None, :]  5.11 us
    unnamed x6, local copies, waits for them, and re-layouts  1.2 us

profile of v2, /device:TPU:0, one launch (start us, length us, event | category | flops | bytes accessed | tf_op | source)
XLA Modules:
  0.0 42.9 jit_solution(15393368662656524475)
XLA Ops:
  0.6 35.9 %both_blocks.1 = (bf16[24,128]{1,0:T(8,128)(2,1)}, f32[12,2,16]{2,1,0:T(2,128)}, f32[2,12,256]{2,1,0:T(8,128)}, f32[2,12,256]{2,1,0:T(8,128)}, f32[2,12,256]{2,1,0:T(8,128)}) custom-call(bf16[24,128]{1,0:T(8,128)(2,1)} %residual_ref.1, f32[2,2048]{1,0:T(2,128)} %gain_ref.1, f32[2,16]{1,0:T(2,128)} %bias_ref.1, f32[2,256]{1,0:T(2,128)} %head_gain_ref.1, ...), custom_call_target="tpu_custom_call" | custom-call | flops 251658240 | bytes 41943040 | tf_op jit(solution)/shard_map/both_blocks/pallas_call | solution.py:457
  36.5 0.0 copy-start.1
  36.5 0.0 copy-start
  36.6 5.1 %multiply_add_fusion = f32[2,12,256,256]{3,2,1,0:T(8,128)} fusion(f32[2,12,256,256]{3,2,1,0:T(8,128)} %mem_hbm.1, f32[2,12,256]{2,1,0:T(8,128)} %get-tuple-element.11, f32[2,12,256]{2,1,0:T(8,128)} %get-tuple-element.10, f32[2,12,256]{2,1,0:T(8,128)} %get-tuple-element.9), kind=kLoop, calls=%fused_computation | loop fusion | flops 4718592 | bytes 12656640 | tf_op jit(solution)/shard_map/add | solution.py:512
  41.7 0.0 copy-done.1
  41.7 0.6 %copy.18 = bf16[24,128]{1,0:T(8,128)(2,1)} copy(bf16[24,128]{1,0:T(8,128)(2,1)S(1)} %copy-done.1) | data formatting | bytes 12288
  42.3 0.0 copy-done
  42.3 0.6 %copy.19 = f32[2,12,16]{2,0,1:T(2,128)} copy(f32[2,12,16]{2,0,1:T(2,128)S(1)} %bitcast.7) | data formatting | bytes 3072
Async XLA Ops:
  36.5 5.1 %copy-start.1 = (bf16[24,128]{1,0:T(8,128)(2,1)S(1)}, bf16[24,128]{1,0:T(8,128)(2,1)}, u32[]{:S(2)}) copy-start(bf16[24,128]{1,0:T(8,128)(2,1)} %get-tuple-element.16) | copy-start | bytes 18436
  36.5 5.7 %copy-start = (f32[12,2,16]{2,1,0:T(2,128)S(1)}, f32[12,2,16]{2,1,0:T(2,128)}, u32[]{:S(2)}) copy-start(f32[12,2,16]{2,1,0:T(2,128)} %get-tuple-element.12) | copy-start | bytes 4612

commit v3 on v2

--- a/solution.py
+++ b/solution.py
@@ -251,7 +251,8 @@
         copies.pop(name).wait()
 
     row_start = pl.multiple_of(core * span, span)
-    for j in range(BLOCKS):
+
+    def fetch_block(j):
         for i, w in enumerate((wq_hbm, wk_hbm, wv_hbm, wo_hbm)):
             fetch(("in", j, i), w.at[j], w_in.at[j, i], w_sem.at[j, i])
         for i, w in enumerate((wi_hbm, wf_hbm)):
@@ -264,6 +265,7 @@
         fetch(("mem", j), mem_hbm.at[j], mem.at[j], mem_sem.at[j])
         fetch(("out", j), wp_hbm.at[j], w_out.at[j], w_sem.at[j, 6])
 
+    fetch_block(0)
     barrier = pltpu.get_barrier_semaphore()
     for step in range(n_tp - 1, 0, -1):
         pl.semaphore_signal(
@@ -297,6 +299,8 @@
             land(("in", j, i))
         for i in range(2):
             land(("gate", j, i))
+        if j + 1 < BLOCKS:
+            fetch_block(j + 1)
         squares = jnp.zeros((seqs, 2 * width), jnp.float32)
         gate_sum = jnp.zeros((seqs, 2 * heads), jnp.float32)
         in_sums = [jnp.zeros((seqs, head_dim), jnp.float32)] * 4
@@ -440,6 +444,22 @@
             out_ref[...] = rounded
     for copy in late_sends:
         copy.wait_send()
+
+
+def update_kernel(
+    keep_ref, value_ref, key_ref, mem_ref, out_in, stab_in, mem_out, out_out, stab_out, column_buf
+):
+    share = keep_ref.shape[1]
+    column_buf[...] = jnp.zeros_like(column_buf)
+    column_buf[:share, :] = value_ref[0]
+    columns = column_buf[...].T
+    for b in range(share):
+        mem_out[0, b] = (
+            keep_ref[0, b : b + 1, :] * mem_ref[0, b]
+            + columns[:, b : b + 1] * key_ref[0, b : b + 1, :]
+        )
+    out_out[...] = out_in[...]
+    stab_out[...] = stab_in[...]
 
 
 def fused_device(n_tp, n_dp, residual_in, norm_gain, w_query, w_key, w_value, w_outgate, w_igate,
@@ -508,9 +528,24 @@
         w_query, w_key, w_value, w_outgate, w_igate.swapaxes(1, 2), w_fgate.swapaxes(1, 2),
         w_proj, mem_matrix,
     )
-    matrix = (
-        keep[:, :, None, :] * mem_matrix + value[:, :, :, None] * key[:, :, None, :]
-    )
+    one_block = lambda *dims: pl.BlockSpec((1,) + dims, lambda j: (j,) + (0,) * len(dims))
+    whole = lambda *dims: pl.BlockSpec(dims, lambda j: (0,) * len(dims))
+    matrix, out, stab_new = pl.pallas_call(
+        update_kernel,
+        grid=(BLOCKS,),
+        out_shape=(
+            jax.ShapeDtypeStruct(mem_matrix.shape, wide),
+            jax.ShapeDtypeStruct(out.shape, low),
+            jax.ShapeDtypeStruct(stab_new.shape, wide),
+        ),
+        in_specs=[one_block(share, head_dim)] * 3
+        + [one_block(share, head_dim, head_dim), whole(*out.shape), whole(*stab_new.shape)],
+        out_specs=(
+            one_block(share, head_dim, head_dim), whole(*out.shape), whole(*stab_new.shape)
+        ),
+        scratch_shapes=[pltpu.VMEM((pad, head_dim), wide)],
+        name="memory_update",
+    )(keep, value, key, mem_matrix, out, stab_new)
     return out, matrix, stab_new.transpose(1, 0, 2)
 
 

time: 43.1 us -> 42.1 us (0.977)
  Pallas kernels: 35.9 us -> 41.1 us
  other arithmetic: 5.11 us -> 0 us
  local copies, waits for them, and re-layouts: 1.2 us -> 0 us
    pallas_call x0 -> x1, Pallas kernels: none -> 5.24 us  [fused_device(): pl.pallas_call(update_kernel, grid=(BLOCKS,), out_shape=(jax.ShapeDtypeSt...]
    add x1 -> x0, other arithmetic: 5.11 us -> none  [fused_device(): keep[:, :, None, :] * mem_matrix + value[:, :, :, None] * key[:, :, None, :]]
    unnamed x6 -> x0, local copies, waits for them, and re-layouts: 1.2 us -> none
where the time goes in v3:
time: 42.1 us; the launch traced here: 41.8 us
  Pallas kernels  41.1 us (98%)
  between operations  0.64 us (2%)
    pallas_call x1, Pallas kernels, fused_device(): pl.pallas_call(functools.partial(fused_kernel, n_tp, n_dp, seqs), out_sha...  35.9 us
    pallas_call x1, Pallas kernels, fused_device(): pl.pallas_call(update_kernel, grid=(BLOCKS,), out_shape=(jax.ShapeDtypeSt...  5.24 us

profile of v3, /device:TPU:0, one launch (start us, length us, event | category | flops | bytes accessed | tf_op | source)
XLA Modules:
  0.0 41.8 jit_solution(1349008288013289603)
XLA Ops:
  0.6 35.9 %both_blocks.1 = (bf16[24,128]{1,0:T(8,128)(2,1)}, f32[12,2,16]{2,1,0:T(2,128)}, f32[2,12,256]{2,1,0:T(8,128)}, f32[2,12,256]{2,1,0:T(8,128)}, f32[2,12,256]{2,1,0:T(8,128)}) custom-call(bf16[24,128]{1,0:T(8,128)(2,1)} %residual_ref.1, f32[2,2048]{1,0:T(2,128)} %gain_ref.1, f32[2,16]{1,0:T(2,128)} %bias_ref.1, f32[2,256]{1,0:T(2,128)} %head_gain_ref.1, ...), custom_call_target="tpu_custom_call" | custom-call | flops 251658240 | bytes 41943040 | tf_op jit(solution)/shard_map/both_blocks/pallas_call | solution.py:477
  36.5 5.2 %memory_update.1 = (f32[2,12,256,256]{3,2,1,0:T(8,128)}, bf16[24,128]{1,0:T(8,128)(2,1)}, f32[12,2,16]{2,1,0:T(2,128)}) custom-call(f32[2,12,256]{2,1,0:T(8,128)} %get-tuple-element.11.keep_ref, f32[2,12,256]{2,1,0:T(8,128)} %get-tuple-element.12.value_ref, f32[2,12,256]{2,1,0:T(8,128)} %get-tuple-element.13.key_ref, f32[2,12,256,256]{3,2,1,0:T(8,128)} %mem_ref.1, ...), custom_call_target="tpu_custom_call" | custom-call | tf_op jit(solution)/shard_map/memory_update/pallas_call | solution.py:533
